TPU v7x, 32 devices: a whole 2x2x4 slice. The times are simulated.
32 devices in a mesh: sp: 8 (over z, y), tp: 4 (over x, core).
Axes of the slice: x: 2, y: 2, z: 4, core: 2. Of those that a mesh axis runs over, the one named last changes fastest.
Arguments:
- inputs: bfloat16 [8192, 2048], P('sp'), may hold values from -6 to 6
- norm_gain: float32 [3, 2048], replicated, may hold values from 0.1 to 1.9
- query_weight: bfloat16 [3, 2048, 1024], P(None, 'sp', 'tp'), may hold values from -64 to 64
- key_weight: bfloat16 [3, 2048, 512], P(None, 'sp', 'tp'), may hold values from -4 to 4
- value_weight: bfloat16 [3, 2048, 512], P(None, 'sp', 'tp'), may hold values from -0.125 to 0.125
- output_weight: bfloat16 [3, 2048, 1024], P(None, 'sp', 'tp'), may hold values from -0.1875 to 0.1875
- sink_logit: float32 [3, 16], P(None, 'tp'), may hold values from 2 to 7
- final_gain: float32 [2048], replicated, may hold values from 0.1 to 1.9
Outputs:
- result: float32 [8192, 2048], P(('sp', 'tp'))
All inputs are finite; a program needn't handle non-finite values.
Results may differ from a plain program's by a relative error of at most 0.015.
Values may be sent and summed in bfloat16 or wider, within the bound.
A program may use at most 64 MiB of HBM per device.

v0:
```python
import jax
import jax.numpy as jnp
from jax import lax
from jax.sharding import PartitionSpec as P

D = 2048
HEAD_DIM = 64
WINDOW = 128
LAYERS = 3
EPS = 1e-06


def extended_2(block, sides, width):
    for axis, dim in sides:
        count = lax.axis_size(axis)
        forward = [(i, i + 1) for i in range(count - 1)]
        backward = [(target, source) for source, target in forward]
        low = lax.ppermute(
            lax.slice_in_dim(block, block.shape[dim] - width, None, axis=dim), axis, forward
        )
        high = lax.ppermute(lax.slice_in_dim(block, 0, width, axis=dim), axis, backward)
        block = jnp.concatenate([low, block, high], axis=dim)
    return block


def norm_rows(values, gain):
    wide_values = values.astype(jnp.float32)
    inv_root = lax.rsqrt(jnp.mean(wide_values * wide_values, axis=-1, keepdims=True) + EPS)
    return wide_values * inv_root * gain


def rotate(values, places):
    half_dim = values.shape[-1] // 2
    inverse = 10000.0 ** (-jnp.arange(half_dim).astype(jnp.float32) / half_dim)
    angles = places[:, None] * inverse[None, :]
    cosine_table = jnp.cos(angles)[:, None, :]
    sine_table = jnp.sin(angles)[:, None, :]
    front_half = values[..., :half_dim]
    back_half = values[..., half_dim:]
    return jnp.concatenate(
        [
            front_half * cosine_table - back_half * sine_table,
            back_half * cosine_table + front_half * sine_table,
        ],
        axis=-1,
    )


def attend(queries, key_rows, value_rows, sink_row, allowed):
    scores = jnp.einsum(
        "qkgd,skd->kgqs", queries, key_rows, preferred_element_type=jnp.float32
    ) * queries.shape[-1] ** (-0.5)
    scores = jnp.where(allowed[None, None], scores, -jnp.inf)
    sink_col = sink_row[:, :, None]
    largest = jnp.maximum(jnp.max(scores, axis=-1), sink_col)
    powers = jnp.exp(scores - largest[..., None])
    denominator = jnp.sum(powers, axis=-1) + jnp.exp(sink_col - largest)
    weights = (powers / denominator[..., None]).astype(jnp.bfloat16)
    blended = jnp.einsum("kgqs,skd->qkgd", weights, value_rows, preferred_element_type=jnp.float32)
    return blended.astype(jnp.bfloat16)


def shards(
    inputs, norm_gain, query_weight, key_weight, value_weight, output_weight, sink_logit, final_gain
):
    tokens = inputs.shape[0]
    local_heads = query_weight.shape[2] // HEAD_DIM
    local_groups = key_weight.shape[2] // HEAD_DIM
    per_group = local_heads // local_groups
    kv_cols = local_groups * HEAD_DIM
    offset = lax.axis_index("sp") * tokens
    seq_total = tokens * lax.axis_size("sp")
    query_pos = offset + jnp.arange(tokens, dtype=jnp.int32)
    places = query_pos.astype(jnp.float32)
    key_pos = offset - WINDOW + jnp.arange(tokens + 2 * WINDOW, dtype=jnp.int32)
    allowed = (
        (jnp.abs(key_pos[None, :] - query_pos[:, None]) <= WINDOW)
        & (key_pos[None, :] >= 0)
        & (key_pos[None, :] < seq_total)
    )
    whole_query, whole_key, whole_value, whole_out = (
        lax.all_gather(query_weight, "sp", axis=1, tiled=True),
        lax.all_gather(key_weight, "sp", axis=1, tiled=True),
        lax.all_gather(value_weight, "sp", axis=1, tiled=True),
        lax.all_gather(output_weight, "sp", axis=1, tiled=True),
    )
    current = inputs
    final_rows = inputs
    for layer in range(LAYERS):
        normed = norm_rows(current, norm_gain[layer]).astype(jnp.bfloat16)
        query_raw = jnp.dot(normed, whole_query[layer], preferred_element_type=jnp.float32)
        key_raw = jnp.dot(normed, whole_key[layer], preferred_element_type=jnp.float32)
        value_raw = jnp.dot(normed, whole_value[layer], preferred_element_type=jnp.float32)
        out_weight = whole_out[layer]
        queries = rotate(
            (query_raw * float(D) ** (-0.5)).reshape(tokens, local_heads, HEAD_DIM), places
        ).astype(jnp.bfloat16)
        key_rot = rotate(
            (key_raw * float(D) ** (-0.5)).reshape(tokens, local_groups, HEAD_DIM), places
        ).astype(jnp.bfloat16)
        packed = jnp.concatenate(
            [key_rot.reshape(tokens, kv_cols), value_raw.astype(jnp.bfloat16)], axis=1
        )
        extended = extended_2(packed, (("sp", 0),), WINDOW)
        key_rows = extended[:, :kv_cols].reshape(-1, local_groups, HEAD_DIM)
        value_all = extended[:, kv_cols:].reshape(-1, local_groups, HEAD_DIM)
        sink_row = sink_logit[layer].reshape(local_groups, per_group)
        attended = attend(
            queries.reshape(tokens, local_groups, per_group, HEAD_DIM),
            key_rows,
            value_all,
            sink_row,
            allowed,
        )
        attended = attended.reshape(tokens, local_heads * HEAD_DIM)

        def project():
            return lax.dot_general(
                attended, out_weight, (((1,), (1,)), ((), ())), preferred_element_type=jnp.float32
            )

        if layer < LAYERS - 1:
            share_rows = lax.psum_scatter(project(), "tp", scatter_dimension=0, tiled=True).astype(
                jnp.bfloat16
            )
            current = lax.all_gather(share_rows, "tp", axis=0, tiled=True)
        else:
            final_rows = lax.psum_scatter(
                project().astype(jnp.bfloat16), "tp", scatter_dimension=0, tiled=True
            )
    return norm_rows(final_rows, final_gain)


def solution(mesh):
    in_specs = (
        P("sp", None),
        P(),
        P(None, "sp", "tp"),
        P(None, "sp", "tp"),
        P(None, "sp", "tp"),
        P(None, "sp", "tp"),
        P(None, "tp"),
        P(),
    )
    out_specs = P(("sp", "tp"), None)
    return jax.shard_map(shards, mesh=mesh, in_specs=in_specs, out_specs=out_specs, check_vma=False)
```

profile of v0, /device:TPU:0, one launch (start us, length us, event | category | flops | bytes accessed | tf_op | source)
XLA Modules:
  0.0 580.5 jit_solution(9668719352871353835)
XLA Ops:
  6.5 0.7 all-gather.7.cloned.1.call-update
  7.3 0.7 all-gather.9.cloned.1.call-update
  8.1 0.7 all-gather.11.cloned.1.call-update
  8.8 0.5 all-gather.13.cloned.1.call-update
  9.4 1.0 fusion.54
  10.4 3.3 fusion.9
  13.8 3.0 fusion.11
  16.7 0.5 multiply_cosine_fusion
  17.3 2.3 fusion.19
  19.5 37.0 %all-gather.7.cloned.1.call-done = bf16[3,2048,128]{2,1,0:T(8,128)(2,1)} async-done(((bf16[3,256,128]{2,1,0:T(8,128)(2,1)}), bf16[3,2048,128]{2,1,0:T(8,128)(2,1)}) %all-gather.7.cloned.1.call-update) | async-done | bytes 1572880 | tf_op jit(solution)/shard_map/all_gather | solution.py:83
  56.5 3.8 convolution_multiply_fusion.5
  60.4 40.8 %all-gather.9.cloned.1.call-done = bf16[3,2048,128]{2,1,0:T(8,128)(2,1)} async-done(((bf16[3,256,128]{2,1,0:T(8,128)(2,1)}), bf16[3,2048,128]{2,1,0:T(8,128)(2,1)}) %all-gather.9.cloned.1.call-update) | async-done | bytes 1572880 | tf_op jit(solution)/shard_map/all_gather | solution.py:84
  101.3 3.8 convolution_convert_fusion.3
  105.1 1.3 collective-permute-start.1
  106.4 5.0 collective-permute-start
  111.6 2.7 collective-permute-done
  114.4 48.1 %all-gather.11.cloned.1.call-done = bf16[3,2048,256]{2,1,0:T(8,128)(2,1)} async-done(((bf16[3,256,256]{2,1,0:T(8,128)(2,1)}), bf16[3,2048,256]{2,1,0:T(8,128)(2,1)}) %all-gather.11.cloned.1.call-update) | async-done | bytes 3145744 | tf_op jit(solution)/shard_map/all_gather | solution.py:82
  162.4 3.8 convolution_multiply_fusion.2
  166.2 0.2 subtract_convert_fusion.2
  166.4 3.7 fusion.3
  170.2 4.7 fusion
  174.8 0.1 exponential_add_fusion.2
  174.9 6.2 %fusion.24 = bf16[2,64,2,1024]{3,1,2,0:T(8,128)(2,1)S(1)} fusion(bf16[1280,2,64,1]{0,2,3,1:T(8,128)(2,1)S(1)} %bitcast.159, f32[2,1280,1024,2]{2,1,3,0:T(8,128)S(1)} %get-tuple-element.38, f32[2,2,1024]{2,1,0:T(2,128)S(1)} %exponential_add_fusion.2, f32[2,2,1024]{2,1,0:T(2,128)S(1)} %broadcast_maximum_fusion.2, pred[1024,1280]{0,1:T(8,128)(4,1)S(1)} %fusion.19), kind=kOutput, calls=%fused_computation.46 | convolution fusion | flops 697565184 | bytes 23166976 | tf_op jit(solution)/shard_map/kgqs,skd->qkgd/dot_general | solution.py:59
  181.1 42.1 %all-gather.13.cloned.1.call-done = bf16[3,2048,256]{2,1,0:T(8,128)(2,1)} async-done(((bf16[3,256,256]{2,1,0:T(8,128)(2,1)}), bf16[3,2048,256]{2,1,0:T(8,128)(2,1)}) %all-gather.13.cloned.1.call-update) | async-done | bytes 3145744 | tf_op jit(solution)/shard_map/all_gather | solution.py:85
  223.2 5.8 fusion.26
  229.1 70.2 %reduce-scatter.4.cloned.1.call-done = f32[256,2048]{1,0:T(8,128)} async-done(((f32[1024,2048]{1,0:T(8,128)}), f32[256,2048]{1,0:T(8,128)}) %reduce-scatter.4.cloned.1.call-update) | async-done | bytes 2097168 | tf_op jit(solution)/shard_map/reduce_scatter | solution.py:123
  299.2 2.7 convert_element_type.115
  302.0 0.2 reduce-scatter.6.cloned.1.call-start
  302.3 34.3 %all-gather.15.cloned.1.call-done = bf16[1024,2048]{1,0:T(8,128)(2,1)} async-done(((bf16[256,2048]{1,0:T(8,128)(2,1)}), bf16[1024,2048]{1,0:T(8,128)(2,1)}) %all-gather.15.cloned.1.call-update) | async-done | bytes 4194320 | tf_op jit(solution)/shard_map/all_gather | solution.py:126
  336.6 3.2 fusion.12
  339.8 0.2 copy-done.2
  340.1 1.0 fusion.14
  341.1 2.7 convolution_multiply_fusion.4
  343.9 1.5 convolution_convert_fusion.2
  345.5 1.3 collective-permute-start.3
  346.8 4.5 collective-permute-start.2
  351.3 2.5 convolution_multiply_fusion.1
  353.9 0.2 subtract_convert_fusion.1
  354.1 0.8 fusion.52
  354.9 3.7 fusion.4
  358.7 4.7 fusion.1
  363.3 0.1 exponential_add_fusion.1
  363.4 7.8 %fusion.23 = bf16[2,64,2,1024]{3,1,2,0:T(8,128)(2,1)} fusion(bf16[1280,2,64,1]{0,2,3,1:T(8,128)(2,1)} %bitcast.161, f32[2,1280,1024,2]{2,1,3,0:T(8,128)S(1)} %get-tuple-element.40, f32[2,2,1024]{2,1,0:T(2,128)S(1)} %exponential_add_fusion.1, f32[2,2,1024]{2,1,0:T(2,128)S(1)} %broadcast_maximum_fusion.1, pred[1024,1280]{0,1:T(8,128)(4,1)S(1)} %fusion.19), kind=kOutput, calls=%fused_computation.45 | convolution fusion | flops 697565184 | bytes 23166976 | tf_op jit(solution)/shard_map/kgqs,skd->qkgd/dot_general | solution.py:59
  371.2 5.9 %fusion.25 = f32[1024,2048]{1,0:T(8,128)} fusion(bf16[1024,256]{0,1:T(8,128)(2,1)} %bitcast.158, bf16[3,2048,256]{2,1,0:T(8,128)(2,1)} %all-gather.13.cloned.1.call-done), kind=kOutput, calls=%fused_computation.56 | convolution fusion | flops 1073741824 | bytes 9961472 | tf_op jit(solution)/shard_map/dot_general | solution.py:118
  377.2 72.4 %reduce-scatter.6.cloned.1.call-done = f32[256,2048]{1,0:T(8,128)} async-done(((f32[1024,2048]{1,0:T(8,128)}), f32[256,2048]{1,0:T(8,128)}) %reduce-scatter.6.cloned.1.call-update) | async-done | bytes 2097168 | tf_op jit(solution)/shard_map/reduce_scatter | solution.py:123
  449.7 2.7 convert_element_type.123
  452.4 0.3 reduce-scatter.8.cloned.1.call-start
  452.7 34.3 %all-gather.17.cloned.1.call-done = bf16[1024,2048]{1,0:T(8,128)(2,1)} async-done(((bf16[256,2048]{1,0:T(8,128)(2,1)}), bf16[1024,2048]{1,0:T(8,128)(2,1)}) %all-gather.17.cloned.1.call-update) | async-done | bytes 4194320 | tf_op jit(solution)/shard_map/all_gather | solution.py:126
  487.0 3.2 fusion.15
  490.3 0.2 copy-done.1
  490.5 1.0 fusion.17
  491.5 2.6 convolution_multiply_fusion.3
  494.2 1.5 convolution_convert_fusion.1
  495.7 1.3 collective-permute-start.5
  497.0 4.5 collective-permute-start.4
  501.6 2.5 convolution_multiply_fusion
  504.2 0.2 subtract_convert_fusion
  504.5 3.7 fusion.5
  508.2 4.7 fusion.2
  513.0 6.2 %fusion.22 = bf16[2,64,2,1024]{3,1,2,0:T(8,128)(2,1)S(1)} fusion(bf16[1280,2,64,1]{0,2,3,1:T(8,128)(2,1)S(1)} %bitcast.160, f32[2,1280,1024,2]{2,1,3,0:T(8,128)S(1)} %get-tuple-element.42, f32[2,2,1024]{2,1,0:T(2,128)S(1)} %exponential_add_fusion, f32[2,2,1024]{2,1,0:T(2,128)S(1)} %broadcast_maximum_fusion, pred[1024,1280]{0,1:T(8,128)(4,1)S(1)} %fusion.19), kind=kOutput, calls=%fused_computation.44 | convolution fusion | flops 697565184 | bytes 23166976 | tf_op jit(solution)/shard_map/kgqs,skd->qkgd/dot_general | solution.py:59
  519.2 4.5 convolution_convert_fusion
  523.7 45.7 %reduce-scatter.8.cloned.1.call-done = bf16[256,2048]{1,0:T(8,128)(2,1)} async-done(((bf16[1024,2048]{1,0:T(8,128)(2,1)}), bf16[256,2048]{1,0:T(8,128)(2,1)}) %reduce-scatter.8.cloned.1.call-update) | async-done | bytes 1048592 | tf_op jit(solution)/shard_map/reduce_scatter | solution.py:128
  569.4 1.5 fusion.20
  570.9 2.8 fusion.21
  (57 shorter events, 1.6 us)
Async XLA Ops:
  6.5 50.0 %all-gather.7.cloned.1.call-start = ((), (), s32[]{:S(2)}) async-start(), calls=%async_computation.3 | async-start | bytes 1769472 | tf_op jit(solution)/shard_map/all_gather | solution.py:83
  7.3 94.0 %all-gather.9.cloned.1.call-start = ((), (), s32[]{:S(2)}) async-start(), calls=%async_computation.4 | async-start | bytes 1769472 | tf_op jit(solution)/shard_map/all_gather | solution.py:84
  8.0 154.4 %all-gather.11.cloned.1.call-start = ((), (), s32[]{:S(2)}) async-start(), calls=%async_computation.5 | async-start | bytes 3538944 | tf_op jit(solution)/shard_map/all_gather | solution.py:82
  8.7 214.5 %all-gather.13.cloned.1.call-start = ((), (), s32[]{:S(2)}) async-start(), calls=%async_computation.6 | async-start | bytes 3538944 | tf_op jit(solution)/shard_map/all_gather | solution.py:85
  9.3 289.9 %reduce-scatter.4.cloned.1.call-start = ((), (), s32[]{:S(2)}) async-start(), calls=%async_computation.7 | async-start | bytes 10485760 | tf_op jit(solution)/shard_map/reduce_scatter | solution.py:123
  9.4 4.4 copy-start
  19.5 91.9 %copy-start.5 = (f32[3,4]{1,0:T(4,128)S(1)}, f32[3,4]{1,0:T(4,128)}, u32[]{:S(2)}) copy-start(f32[3,4]{1,0:T(4,128)} %param.14) | copy-start | bytes 148
  105.1 6.4 %collective-permute-start.1 = (bf16[128,256]{0,1:T(8,128)(2,1)S(1)}, bf16[128,256]{0,1:T(8,128)(2,1)S(1)}, u32[]{:S(2)}, u32[]{:S(2)}) collective-permute-start(bf16[128,256]{0,1:T(8,128)(2,1)S(1)} %get-tuple-element.31), channel_id=1, source_target_pairs={{4,0},{8,4},{12,8},{16,12},{20,16},{24,20},{28,24},{5,1},{9,5},{13... | collective-permute-start | bytes 196616 | tf_op jit(solution)/shard_map/ppermute | solution.py:21
  106.4 7.8 %collective-permute-start = (bf16[128,256]{0,1:T(8,128)(2,1)S(1)}, bf16[128,256]{0,1:T(8,128)(2,1)S(1)}, u32[]{:S(2)}, u32[]{:S(2)}) collective-permute-start(bf16[128,256]{0,1:T(8,128)(2,1)S(1)} %get-tuple-element.30), channel_id=1, source_target_pairs={{0,4},{4,8},{8,12},{12,16},{16,20},{20,24},{24,28},{1,5},{5,9},{9,... | collective-permute-start | bytes 196616 | tf_op jit(solution)/shard_map/ppermute | solution.py:18
  229.0 107.6 %all-gather.15.cloned.1.call-start = ((), (), s32[]{:S(2)}) async-start(), calls=%async_computation.8 | async-start | bytes 5242880 | tf_op jit(solution)/shard_map/all_gather | solution.py:126
  302.0 147.7 %reduce-scatter.6.cloned.1.call-start = ((), (), s32[]{:S(2)}) async-start(), calls=%async_computation.9 | async-start | bytes 10485760 | tf_op jit(solution)/shard_map/reduce_scatter | solution.py:123
  336.6 3.4 copy-start.2
  341.1 2.8 copy-start.3
  345.5 8.6 %collective-permute-start.3 = (bf16[128,256]{0,1:T(8,128)(2,1)S(1)}, bf16[128,256]{0,1:T(8,128)(2,1)S(1)}, u32[]{:S(2)}, u32[]{:S(2)}) collective-permute-start(bf16[128,256]{0,1:T(8,128)(2,1)S(1)} %get-tuple-element.29), channel_id=1, source_target_pairs={{4,0},{8,4},{12,8},{16,12},{20,16},{24,20},{28,24},{5,1},{9,5},{13... | collective-permute-start | bytes 196616 | tf_op jit(solution)/shard_map/ppermute | solution.py:21
  346.8 7.3 %collective-permute-start.2 = (bf16[128,256]{0,1:T(8,128)(2,1)S(1)}, bf16[128,256]{0,1:T(8,128)(2,1)S(1)}, u32[]{:S(2)}, u32[]{:S(2)}) collective-permute-start(bf16[128,256]{0,1:T(8,128)(2,1)S(1)} %get-tuple-element.28), channel_id=1, source_target_pairs={{0,4},{4,8},{8,12},{12,16},{16,20},{20,24},{24,28},{1,5},{5,9},{9,... | collective-permute-start | bytes 196616 | tf_op jit(solution)/shard_map/ppermute | solution.py:18
  377.2 109.8 %all-gather.17.cloned.1.call-start = ((), (), s32[]{:S(2)}) async-start(), calls=%async_computation.10 | async-start | bytes 5242880 | tf_op jit(solution)/shard_map/all_gather | solution.py:126
  452.4 117.0 %reduce-scatter.8.cloned.1.call-start = ((), (), s32[]{:S(2)}) async-start(), calls=%async_computation.11 | async-start | bytes 5242880 | tf_op jit(solution)/shard_map/reduce_scatter | solution.py:128
  487.0 3.4 copy-start.1
  495.7 8.6 %collective-permute-start.5 = (bf16[128,256]{0,1:T(8,128)(2,1)S(1)}, bf16[128,256]{0,1:T(8,128)(2,1)S(1)}, u32[]{:S(2)}, u32[]{:S(2)}) collective-permute-start(bf16[128,256]{0,1:T(8,128)(2,1)S(1)} %get-tuple-element.27), channel_id=1, source_target_pairs={{4,0},{8,4},{12,8},{16,12},{20,16},{24,20},{28,24},{5,1},{9,5},{13... | collective-permute-start | bytes 196616 | tf_op jit(solution)/shard_map/ppermute | solution.py:21
  497.0 7.3 %collective-permute-start.4 = (bf16[128,256]{0,1:T(8,128)(2,1)S(1)}, bf16[128,256]{0,1:T(8,128)(2,1)S(1)}, u32[]{:S(2)}, u32[]{:S(2)}) collective-permute-start(bf16[128,256]{0,1:T(8,128)(2,1)S(1)} %get-tuple-element.26), channel_id=1, source_target_pairs={{0,4},{4,8},{8,12},{12,16},{16,20},{20,24},{24,28},{1,5},{5,9},{9,... | collective-permute-start | bytes 196616 | tf_op jit(solution)/shard_map/ppermute | solution.py:18
  519.2 51.7 %copy-start.4 = (f32[2048]{0:T(1024)S(1)}, f32[2048]{0:T(1024)}, u32[]{:S(2)}) copy-start(f32[2048]{0:T(1024)} %param.15) | copy-start | bytes 24580
Sparse Core Ops, SparseCore 0:
  9.5 46.9 all-gather.6
  58.7 42.5 all-gather.8
  103.5 58.9 all-gather.10
  164.5 58.7 all-gather.12
  229.2 70.0 reduce-scatter.3
  302.1 34.4 all-gather.14
  377.3 72.3 reduce-scatter.5
  452.5 34.4 all-gather.16
  523.9 45.4 reduce-scatter.7
where the time goes:
time: 586 us; the launch traced here: 581 us
  waiting for transfers between devices  430 us (73%)
  matrix products  72.3 us (12%)
  other arithmetic  42.9 us (7%)
  starting transfers between devices  18.7 us (3%)
  between operations  13.9 us (2%)
    reduce_scatter x2, waiting for transfers between devices, shards(): lax.psum_scatter(project(), 'tp', scatter_dimension=0, tiled=True)  143 us
    all_gather x2, waiting for transfers between devices, shards(): current = lax.all_gather(share_rows, 'tp', axis=0, tiled=True)  68.6 us
    all_gather x1, waiting for transfers between devices, shards(): lax.all_gather(query_weight, 'sp', axis=1, tiled=True)  48.1 us
    reduce_scatter x1, waiting for transfers between devices, shards(): lax.psum_scatter(project().astype(jnp.bfloat16), 'tp', scatter_dimension=...  45.7 us
    all_gather x1, waiting for transfers between devices, shards(): lax.all_gather(output_weight, 'sp', axis=1, tiled=True)  42.1 us
    all_gather x1, waiting for transfers between devices, shards(): lax.all_gather(value_weight, 'sp', axis=1, tiled=True)  40.8 us
    all_gather x1, waiting for transfers between devices, shards(): lax.all_gather(key_weight, 'sp', axis=1, tiled=True)  37 us
    dot_general x3, matrix products, attend(): jnp.einsum('kgqs,skd->qkgd', weights, value_rows, preferred_element_type=...  20.2 us
  transfers between devices with their start and end apart: 15, of which 10 were waited for; matrix products, arithmetic and copies ran while one was open for 7% of the time, Pallas kernels for 0%

commit v1 on v0

--- a/solution.py
+++ b/solution.py
@@ -78,11 +78,15 @@
         & (key_pos[None, :] >= 0)
         & (key_pos[None, :] < seq_total)
     )
+
+    def manage_slot_all(payload):
+        return jnp.concatenate(lax.all_gather(payload, axis_name="sp"), axis=1)
+
     whole_query, whole_key, whole_value, whole_out = (
         lax.all_gather(query_weight, "sp", axis=1, tiled=True),
         lax.all_gather(key_weight, "sp", axis=1, tiled=True),
         lax.all_gather(value_weight, "sp", axis=1, tiled=True),
-        lax.all_gather(output_weight, "sp", axis=1, tiled=True),
+        manage_slot_all(output_weight),
     )
     current = inputs
     final_rows = inputs

time: 586 us -> 598 us (1.020)
  transfers between devices with their start and end apart: 15 -> 15, of which waited for: 10 -> 10; matrix products, arithmetic and copies ran while one was open for 7% -> 6% of each run, Pallas kernels for 0% -> 0%
where the time goes in v1:
time: 598 us; the launch traced here: 593 us
  waiting for transfers between devices  434 us (73%)
  matrix products  74.8 us (13%)
  other arithmetic  43.5 us (7%)
  starting transfers between devices  18.7 us (3%)
  between operations  13.9 us (2%)
  local copies, waits for them, and re-layouts  8.21 us (1%)
    reduce_scatter x2, waiting for transfers between devices, shards(): lax.psum_scatter(project(), 'tp', scatter_dimension=0, tiled=True)  143 us
    all_gather x2, waiting for transfers between devices, shards(): current = lax.all_gather(share_rows, 'tp', axis=0, tiled=True)  68.6 us
    all_gather x1, waiting for transfers between devices, shards(): lax.all_gather(query_weight, 'sp', axis=1, tiled=True)  48.1 us
    all_gather x1, waiting for transfers between devices, manage_slot_all(): return jnp.concatenate(lax.all_gather(payload, axis_name='sp'), axis=1)  45.9 us
    reduce_scatter x1, waiting for transfers between devices, shards(): lax.psum_scatter(project().astype(jnp.bfloat16), 'tp', scatter_dimension=...  45.7 us
    all_gather x1, waiting for transfers between devices, shards(): lax.all_gather(value_weight, 'sp', axis=1, tiled=True)  40.8 us
    all_gather x1, waiting for transfers between devices, shards(): lax.all_gather(key_weight, 'sp', axis=1, tiled=True)  36.9 us
    dot_general x3, matrix products, attend(): jnp.einsum('kgqs,skd->qkgd', weights, value_rows, preferred_element_type=...  24.7 us
  transfers between devices with their start and end apart: 15, of which 10 were waited for; matrix products, arithmetic and copies ran while one was open for 6% of the time, Pallas kernels for 0%

profile of v1, /device:TPU:0, one launch (start us, length us, event | category | flops | bytes accessed | tf_op | source)
XLA Modules:
  0.0 593.0 jit_solution(16524265368742153774)
XLA Ops:
  6.5 0.7 all-gather.8.cloned.1.call-update
  7.3 0.7 all-gather.10.cloned.1.call-update
  8.1 0.7 all-gather.12.cloned.1.call-update
  8.8 0.5 all-gather.18.cloned.1.call-update
  9.4 1.0 fusion.53
  10.4 3.3 fusion.9
  13.8 3.0 fusion.11
  16.7 0.5 multiply_cosine_fusion
  17.3 2.3 fusion.19
  19.6 36.9 %all-gather.8.cloned.1.call-done = bf16[3,2048,128]{2,1,0:T(8,128)(2,1)} async-done(((bf16[3,256,128]{2,1,0:T(8,128)(2,1)}), bf16[3,2048,128]{2,1,0:T(8,128)(2,1)}) %all-gather.8.cloned.1.call-update) | async-done | bytes 1572880 | tf_op jit(solution)/shard_map/all_gather | solution.py:87
  56.5 3.8 convolution_multiply_fusion.5
  60.4 40.8 %all-gather.10.cloned.1.call-done = bf16[3,2048,128]{2,1,0:T(8,128)(2,1)} async-done(((bf16[3,256,128]{2,1,0:T(8,128)(2,1)}), bf16[3,2048,128]{2,1,0:T(8,128)(2,1)}) %all-gather.10.cloned.1.call-update) | async-done | bytes 1572880 | tf_op jit(solution)/shard_map/all_gather | solution.py:88
  101.3 3.8 convolution_convert_fusion.3
  105.1 1.3 collective-permute-start.1
  106.4 5.0 collective-permute-start
  111.6 2.7 collective-permute-done
  114.3 48.1 %all-gather.12.cloned.1.call-done = bf16[3,2048,256]{2,1,0:T(8,128)(2,1)} async-done(((bf16[3,256,256]{2,1,0:T(8,128)(2,1)}), bf16[3,2048,256]{2,1,0:T(8,128)(2,1)}) %all-gather.12.cloned.1.call-update) | async-done | bytes 3145744 | tf_op jit(solution)/shard_map/all_gather | solution.py:86
  162.4 3.8 convolution_multiply_fusion.2
  166.2 0.2 subtract_convert_fusion.2
  166.4 3.6 fusion.3
  170.1 4.6 fusion
  174.7 2.5 copy-done
  177.3 45.9 %all-gather.18.cloned.1.call-done = bf16[24,256,256]{2,1,0:T(8,128)(2,1)} async-done(((bf16[3,256,256]{2,1,0:T(8,128)(2,1)}), bf16[24,256,256]{2,1,0:T(8,128)(2,1)}) %all-gather.18.cloned.1.call-update) | async-done | bytes 3145744 | tf_op jit(solution)/shard_map/all_gather | solution.py:83
  223.2 3.1 fusion.49
  226.3 10.6 %fusion.24 = bf16[2,64,2,1024]{3,1,2,0:T(8,128)(2,1)S(1)} fusion(bf16[1280,2,64,1]{0,2,3,1:T(8,128)(2,1)S(1)} %bitcast.163, f32[2,1280,1024,2]{2,1,3,0:T(8,128)} %copy-done, f32[2,2,1024]{2,1,0:T(2,128)S(1)} %exponential_add_fusion.2, f32[2,2,1024]{2,1,0:T(2,128)S(1)} %broadcast_maximum_fusion.2, pred[1024,1280]{0,1:T(8,128)(4,1)S(1)} %fusion.19), kind=kOutput, calls=%fused_computation.46 | convolution fusion | flops 697565184 | bytes 23166976 | tf_op jit(solution)/shard_map/kgqs,skd->qkgd/dot_general | solution.py:59
  236.9 4.5 fusion.54
  241.5 70.2 %reduce-scatter.4.cloned.1.call-done = f32[256,2048]{1,0:T(8,128)} async-done(((f32[1024,2048]{1,0:T(8,128)}), f32[256,2048]{1,0:T(8,128)}) %reduce-scatter.4.cloned.1.call-update) | async-done | bytes 2097168 | tf_op jit(solution)/shard_map/reduce_scatter | solution.py:127
  311.7 2.8 convert_element_type.115
  314.4 0.2 reduce-scatter.6.cloned.1.call-start
  314.7 34.3 %all-gather.14.cloned.1.call-done = bf16[1024,2048]{1,0:T(8,128)(2,1)} async-done(((bf16[256,2048]{1,0:T(8,128)(2,1)}), bf16[1024,2048]{1,0:T(8,128)(2,1)}) %all-gather.14.cloned.1.call-update) | async-done | bytes 4194320 | tf_op jit(solution)/shard_map/all_gather | solution.py:130
  349.1 3.2 fusion.12
  352.3 0.2 copy-done.3
  352.5 1.0 fusion.14
  353.5 2.6 convolution_multiply_fusion.4
  356.2 2.6 convolution_convert_fusion.2
  358.8 1.3 collective-permute-start.3
  360.1 4.5 collective-permute-start.2
  364.7 2.5 convolution_multiply_fusion.1
  367.5 0.8 fusion.51
  368.2 3.7 fusion.4
  372.0 4.7 fusion.1
  376.8 7.2 %fusion.23 = bf16[2,64,2,1024]{3,1,2,0:T(8,128)(2,1)S(1)} fusion(bf16[1280,2,64,1]{0,2,3,1:T(8,128)(2,1)} %bitcast.165, f32[2,1280,1024,2]{2,1,3,0:T(8,128)S(1)} %get-tuple-element.43, f32[2,2,1024]{2,1,0:T(2,128)S(1)} %exponential_add_fusion.1, f32[2,2,1024]{2,1,0:T(2,128)S(1)} %broadcast_maximum_fusion.1, pred[1024,1280]{0,1:T(8,128)(4,1)S(1)} %fusion.19), kind=kOutput, calls=%fused_computation.45 | convolution fusion | flops 697565184 | bytes 23166976 | tf_op jit(solution)/shard_map/kgqs,skd->qkgd/dot_general | solution.py:59
  383.9 4.5 fusion.55
  388.5 72.4 %reduce-scatter.6.cloned.1.call-done = f32[256,2048]{1,0:T(8,128)} async-done(((f32[1024,2048]{1,0:T(8,128)}), f32[256,2048]{1,0:T(8,128)}) %reduce-scatter.6.cloned.1.call-update) | async-done | bytes 2097168 | tf_op jit(solution)/shard_map/reduce_scatter | solution.py:127
  461.0 2.8 convert_element_type.123
  463.7 0.3 reduce-scatter.8.cloned.1.call-start
  464.1 34.3 %all-gather.16.cloned.1.call-done = bf16[1024,2048]{1,0:T(8,128)(2,1)} async-done(((bf16[256,2048]{1,0:T(8,128)(2,1)}), bf16[1024,2048]{1,0:T(8,128)(2,1)}) %all-gather.16.cloned.1.call-update) | async-done | bytes 4194320 | tf_op jit(solution)/shard_map/all_gather | solution.py:130
  498.4 3.2 fusion.15
  501.6 0.2 copy-done.2
  501.8 1.0 fusion.17
  502.9 2.6 convolution_multiply_fusion.3
  505.5 2.6 convolution_convert_fusion.1
  508.1 1.3 collective-permute-start.5
  509.4 4.5 collective-permute-start.4
  514.0 2.5 convolution_multiply_fusion
  516.5 0.2 subtract_convert_fusion
  516.8 3.7 fusion.5
  520.6 4.7 fusion.2
  525.3 0.7 exponential_add_fusion
  526.0 6.9 %fusion.22 = bf16[2,64,2,1024]{3,1,2,0:T(8,128)(2,1)S(1)} fusion(bf16[1280,2,64,1]{0,2,3,1:T(8,128)(2,1)S(1)} %bitcast.164, f32[2,1280,1024,2]{2,1,3,0:T(8,128)S(1)} %get-tuple-element.45, f32[2,2,1024]{2,1,0:T(2,128)} %exponential_add_fusion, f32[2,2,1024]{2,1,0:T(2,128)} %copy-done.5, pred[1024,1280]{0,1:T(8,128)(4,1)S(1)} %fusion.19), kind=kOutput, calls=%fused_computation.44 | convolution fusion | flops 697565184 | bytes 23166976 | tf_op jit(solution)/shard_map/kgqs,skd->qkgd/dot_general | solution.py:59
  533.0 3.3 convolution_convert_fusion
  536.3 45.7 %reduce-scatter.8.cloned.1.call-done = bf16[256,2048]{1,0:T(8,128)(2,1)} async-done(((bf16[1024,2048]{1,0:T(8,128)(2,1)}), bf16[256,2048]{1,0:T(8,128)(2,1)}) %reduce-scatter.8.cloned.1.call-update) | async-done | bytes 1048592 | tf_op jit(solution)/shard_map/reduce_scatter | solution.py:132
  581.9 1.5 fusion.20
  583.5 2.8 fusion.21
  (62 shorter events, 1.9 us)
Async XLA Ops:
  6.5 50.0 %all-gather.8.cloned.1.call-start = ((), (), s32[]{:S(2)}) async-start(), calls=%async_computation.3 | async-start | bytes 1769472 | tf_op jit(solution)/shard_map/all_gather | solution.py:87
  7.3 94.0 %all-gather.10.cloned.1.call-start = ((), (), s32[]{:S(2)}) async-start(), calls=%async_computation.4 | async-start | bytes 1769472 | tf_op jit(solution)/shard_map/all_gather | solution.py:88
  8.0 154.4 %all-gather.12.cloned.1.call-start = ((), (), s32[]{:S(2)}) async-start(), calls=%async_computation.5 | async-start | bytes 3538944 | tf_op jit(solution)/shard_map/all_gather | solution.py:86
  8.7 214.4 %all-gather.18.cloned.1.call-start = ((), (), s32[]{:S(2)}) async-start(), calls=%async_computation.11 | async-start | bytes 3538944 | tf_op jit(solution)/shard_map/all_gather | solution.py:83
  9.3 302.3 %reduce-scatter.4.cloned.1.call-start = ((), (), s32[]{:S(2)}) async-start(), calls=%async_computation.6 | async-start | bytes 10485760 | tf_op jit(solution)/shard_map/reduce_scatter | solution.py:127
  9.4 4.4 copy-start.1
  19.5 91.9 %copy-start.7 = (f32[3,4]{1,0:T(4,128)S(1)}, f32[3,4]{1,0:T(4,128)}, u32[]{:S(2)}) copy-start(f32[3,4]{1,0:T(4,128)} %param.14) | copy-start | bytes 148
  105.1 6.4 %collective-permute-start.1 = (bf16[128,256]{0,1:T(8,128)(2,1)S(1)}, bf16[128,256]{0,1:T(8,128)(2,1)S(1)}, u32[]{:S(2)}, u32[]{:S(2)}) collective-permute-start(bf16[128,256]{0,1:T(8,128)(2,1)S(1)} %get-tuple-element.34), channel_id=1, source_target_pairs={{4,0},{8,4},{12,8},{16,12},{20,16},{24,20},{28,24},{5,1},{9,5},{13... | collective-permute-start | bytes 196616 | tf_op jit(solution)/shard_map/ppermute | solution.py:21
  106.4 7.8 %collective-permute-start = (bf16[128,256]{0,1:T(8,128)(2,1)S(1)}, bf16[128,256]{0,1:T(8,128)(2,1)S(1)}, u32[]{:S(2)}, u32[]{:S(2)}) collective-permute-start(bf16[128,256]{0,1:T(8,128)(2,1)S(1)} %get-tuple-element.33), channel_id=1, source_target_pairs={{0,4},{4,8},{8,12},{12,16},{16,20},{20,24},{24,28},{1,5},{5,9},{9,... | collective-permute-start | bytes 196616 | tf_op jit(solution)/shard_map/ppermute | solution.py:18
  170.0 7.2 %copy-start = (f32[2,1280,1024,2]{2,1,3,0:T(8,128)}, f32[2,1280,1024,2]{2,1,3,0:T(8,128)S(1)}, u32[]{:S(2)}) copy-start(f32[2,1280,1024,2]{2,1,3,0:T(8,128)S(1)} %get-tuple-element.41) | copy-start | bytes 62914564
  241.5 107.6 %all-gather.14.cloned.1.call-start = ((), (), s32[]{:S(2)}) async-start(), calls=%async_computation.7 | async-start | bytes 5242880 | tf_op jit(solution)/shard_map/all_gather | solution.py:130
  314.4 146.5 %reduce-scatter.6.cloned.1.call-start = ((), (), s32[]{:S(2)}) async-start(), calls=%async_computation.8 | async-start | bytes 10485760 | tf_op jit(solution)/shard_map/reduce_scatter | solution.py:127
  349.1 3.4 copy-start.3
  358.8 8.6 %collective-permute-start.3 = (bf16[128,256]{0,1:T(8,128)(2,1)S(1)}, bf16[128,256]{0,1:T(8,128)(2,1)S(1)}, u32[]{:S(2)}, u32[]{:S(2)}) collective-permute-start(bf16[128,256]{0,1:T(8,128)(2,1)S(1)} %get-tuple-element.32), channel_id=1, source_target_pairs={{4,0},{8,4},{12,8},{16,12},{20,16},{24,20},{28,24},{5,1},{9,5},{13... | collective-permute-start | bytes 196616 | tf_op jit(solution)/shard_map/ppermute | solution.py:21
  360.1 7.3 %collective-permute-start.2 = (bf16[128,256]{0,1:T(8,128)(2,1)S(1)}, bf16[128,256]{0,1:T(8,128)(2,1)S(1)}, u32[]{:S(2)}, u32[]{:S(2)}) collective-permute-start(bf16[128,256]{0,1:T(8,128)(2,1)S(1)} %get-tuple-element.31), channel_id=1, source_target_pairs={{0,4},{4,8},{8,12},{12,16},{16,20},{20,24},{24,28},{1,5},{5,9},{9,... | collective-permute-start | bytes 196616 | tf_op jit(solution)/shard_map/ppermute | solution.py:18
  388.5 109.9 %all-gather.16.cloned.1.call-start = ((), (), s32[]{:S(2)}) async-start(), calls=%async_computation.9 | async-start | bytes 5242880 | tf_op jit(solution)/shard_map/all_gather | solution.py:130
  463.7 118.2 %reduce-scatter.8.cloned.1.call-start = ((), (), s32[]{:S(2)}) async-start(), calls=%async_computation.10 | async-start | bytes 5242880 | tf_op jit(solution)/shard_map/reduce_scatter | solution.py:132
  498.4 3.4 copy-start.2
  508.1 8.6 %collective-permute-start.5 = (bf16[128,256]{0,1:T(8,128)(2,1)S(1)}, bf16[128,256]{0,1:T(8,128)(2,1)S(1)}, u32[]{:S(2)}, u32[]{:S(2)}) collective-permute-start(bf16[128,256]{0,1:T(8,128)(2,1)S(1)} %get-tuple-element.30), channel_id=1, source_target_pairs={{4,0},{8,4},{12,8},{16,12},{20,16},{24,20},{28,24},{5,1},{9,5},{13... | collective-permute-start | bytes 196616 | tf_op jit(solution)/shard_map/ppermute | solution.py:21
  509.4 7.3 %collective-permute-start.4 = (bf16[128,256]{0,1:T(8,128)(2,1)S(1)}, bf16[128,256]{0,1:T(8,128)(2,1)S(1)}, u32[]{:S(2)}, u32[]{:S(2)}) collective-permute-start(bf16[128,256]{0,1:T(8,128)(2,1)S(1)} %get-tuple-element.29), channel_id=1, source_target_pairs={{0,4},{4,8},{8,12},{12,16},{16,20},{20,24},{24,28},{1,5},{5,9},{9,... | collective-permute-start | bytes 196616 | tf_op jit(solution)/shard_map/ppermute | solution.py:18
  520.6 4.7 copy-start.5
  526.0 7.0 %copy-start.4 = (bf16[1,8,256,256]{3,2,0,1:T(8,128)(2,1)S(1)}, bf16[1,8,256,256]{3,2,0,1:T(8,128)(2,1)}, u32[]{:S(2)}) copy-start(bf16[1,8,256,256]{3,2,0,1:T(8,128)(2,1)} %get-tuple-element.8) | copy-start | bytes 3145732
  533.0 50.5 %copy-start.6 = (f32[2048]{0:T(1024)S(1)}, f32[2048]{0:T(1024)}, u32[]{:S(2)}) copy-start(f32[2048]{0:T(1024)} %param.15) | copy-start | bytes 24580
Sparse Core Ops, SparseCore 0:
  9.5 46.9 all-gather.7
  58.7 42.5 all-gather.9
  103.5 58.9 all-gather.11
  164.5 58.6 all-gather.17
  241.6 70.0 reduce-scatter.3
  314.6 34.4 all-gather.13
  388.6 72.3 reduce-scatter.5
  463.9 34.4 all-gather.15
  536.4 45.5 reduce-scatter.7
